TPU v7x, 32 devices: a whole 2x2x4 slice. The times are simulated.
32 devices in a mesh: ep: 8 (over z, x), tp: 4 (over y, core).
Axes of the slice: x: 2, y: 2, z: 4, core: 2. Of those that a mesh axis runs over, the one named last changes fastest.
Arguments:
- tokens: bfloat16 [128, 1024], P('ep'), may hold values from -6 to 6
- memory: float32 [128, 4, 128, 256], P('ep', 'tp'), may hold values from -6 to 6
- log_scale: float32 [128, 4], P('ep', 'tp'), may hold values from -1 to 130
- mix_gain_in: float32 [1024], replicated, may hold values from 0.1 to 1.9
- w_query: bfloat16 [1024, 512], P(None, 'tp'), may hold values from -0.1875 to 0.1875
- w_key: bfloat16 [1024, 512], P(None, 'tp'), may hold values from -0.1875 to 0.1875
- w_value: bfloat16 [1024, 1024], P(None, 'tp'), may hold values from -0.1875 to 0.1875
- w_igate: bfloat16 [1024, 4], P(None, 'tp'), may hold values from -0.1875 to 0.1875
- w_fgate: bfloat16 [1024, 4], P(None, 'tp'), may hold values from -0.1875 to 0.1875
- igate_bias: float32 [4], P('tp'), may hold values from -1 to 1
- fgate_bias: float32 [4], P('tp'), may hold values from 0 to 4
- head_gain: float32 [1024], P('tp'), may hold values from 0.1 to 1.9
- w_output: bfloat16 [1024, 1024], P('tp'), may hold values from -0.1875 to 0.1875
- mix_gain_out: float32 [1024], replicated, may hold values from 0.1 to 1.9
- ffn_gain_in: float32 [1024], replicated, may hold values from 0.1 to 1.9
- routes: int32 [128, 6], P('ep'), may hold values from 0 to 7, all different within a row; in each aligned block of 16 rows (0 to 15, 16 to 31, ...) at most 16 rows name the same one
- route_weights: float32 [128, 6], P('ep'), may hold values from 0.1 to 1
- expert_gate: bfloat16 [8, 1024, 1024], P('ep', None, 'tp'), may hold values from -0.1875 to 0.1875
- expert_up: bfloat16 [8, 1024, 1024], P('ep', None, 'tp'), may hold values from -0.1875 to 0.1875
- expert_down: bfloat16 [8, 1024, 1024], P('ep', 'tp'), may hold values from -0.9375 to 0.9375
- ffn_gain_out: float32 [1024], P('tp'), may hold values from 0.1 to 1.9
Outputs:
- output: bfloat16 [128, 1024], P('ep', 'tp')
Inputs may be any that keep to these rules, and one draw needn't show every extreme that they name: `routes`: among the 16 tokens of one index of ep no expert is named by more than 16 tokens, and in every draw some expert is named by exactly 16 of them.
All inputs are finite; a program needn't handle non-finite values.
Results may differ from a plain program's by a relative error of at most 0.02.
Values may be sent and summed in bfloat16 or wider, within the bound.
A program may use at most 64 MiB of HBM per device.

v0:
```python
import jax
import jax.numpy as jnp
from jax import lax
from jax.sharding import PartitionSpec as P

EPS = 1e-06


def rms_scale(values):
    return lax.rsqrt(jnp.mean(values * values, axis=-1, keepdims=True) + EPS)


def per_device(
    tokens,
    memory,
    log_scale,
    mix_gain_in,
    w_query,
    w_key,
    w_value,
    w_igate,
    w_fgate,
    igate_bias,
    fgate_bias,
    head_gain,
    w_output,
    mix_gain_out,
    ffn_gain_in,
    routes,
    route_weights,
    expert_gate,
    expert_up,
    expert_down,
    ffn_gain_out,
):
    f32 = jnp.float32
    bf16 = jnp.bfloat16
    seqs, width = tokens.shape
    heads = log_scale.shape[1]
    key_dim = memory.shape[2]
    value_dim = memory.shape[3]
    xf = tokens.astype(f32)
    normed = (xf * rms_scale(xf) * mix_gain_in).astype(bf16)
    query = jnp.dot(normed, w_query, preferred_element_type=f32).reshape(
        seqs, heads, key_dim
    ) * key_dim ** (-0.5)
    keys = jnp.dot(normed, w_key, preferred_element_type=f32).reshape(seqs, heads, key_dim)
    values = jnp.dot(normed, w_value, preferred_element_type=f32).reshape(seqs, heads, value_dim)
    in_pre = jnp.dot(normed, w_igate, preferred_element_type=f32) + igate_bias
    forget_log = jax.nn.log_sigmoid(
        jnp.dot(normed, w_fgate, preferred_element_type=f32) + fgate_bias
    )
    carried = forget_log + log_scale
    new_max = jnp.maximum(carried, in_pre)
    carry_weight = jnp.exp(carried - new_max)
    fresh_weight = jnp.exp(in_pre - new_max)
    recall = jnp.einsum("shk,shkv->shv", query, memory, precision=lax.Precision.HIGHEST)
    match = jnp.sum(query * keys, axis=-1)
    read = carry_weight[..., None] * recall + (fresh_weight * match)[..., None] * values
    headout = (
        (read * rms_scale(read) * head_gain.reshape(heads, value_dim))
        .astype(bf16)
        .reshape(seqs, heads * value_dim)
    )
    partial_value = jnp.dot(headout, w_output, preferred_element_type=f32)
    mixed = lax.psum(partial_value.astype(jnp.bfloat16), "tp").astype(jnp.float32)
    resid = (xf + mixed * rms_scale(mixed) * mix_gain_out).astype(bf16)
    rf = resid.astype(f32)
    ffn_in = (rf * rms_scale(rf) * ffn_gain_in).astype(bf16)
    lanes = lax.axis_size("tp")
    quarter = width // lanes
    own = lax.axis_index("tp") * quarter
    local_experts = expert_gate.shape[0]
    experts_all = local_experts * lax.axis_size("ep")
    top = routes.shape[1]
    cap = min(seqs, max(2, 3 * seqs * top // (2 * experts_all)))
    flat = routes.reshape(-1)
    hits = (flat[:, None] == jnp.arange(experts_all, dtype=jnp.int32)[None, :]).astype(jnp.int32)
    earlier = jnp.cumsum(hits, axis=0) - hits
    slot = jnp.sum(earlier * hits, axis=1)
    place = (flat * cap + slot).reshape(seqs, top)
    picker = jnp.any(
        jnp.arange(experts_all * cap, dtype=jnp.int32)[:, None, None] == place[None, :, :], axis=2
    ).astype(bf16)
    outbound = (
        jnp.dot(picker, ffn_in, preferred_element_type=f32)
        .astype(bf16)
        .reshape(experts_all, cap, width)
    )
    arrived = lax.all_to_all(outbound, "ep", split_axis=0, concat_axis=0, tiled=True)
    items = arrived.shape[1]
    rows = arrived.reshape(-1, local_experts, items, width)
    gate = jnp.einsum("secd,edf->secf", rows, expert_gate, preferred_element_type=f32)
    up = jnp.einsum("secd,edf->secf", rows, expert_up, preferred_element_type=f32)
    act = (jax.nn.silu(gate) * up).astype(bf16)
    part = jnp.einsum("secf,efd->secd", act, expert_down, preferred_element_type=f32).reshape(
        -1, items, width
    )
    summed = lax.psum_scatter(
        part.astype(jnp.bfloat16), "tp", scatter_dimension=2, tiled=True
    ).astype(jnp.float32)
    done = summed.astype(bf16)
    returned = lax.all_to_all(done, "ep", split_axis=0, concat_axis=0, tiled=True)
    columns = returned.shape[2]
    chosen = jnp.take(returned.reshape(-1, columns), place.reshape(-1), axis=0).reshape(
        seqs, top, columns
    )
    routed = jnp.sum(route_weights[:, :, None] * chosen.astype(f32), axis=1)
    resid_part = lax.dynamic_slice_in_dim(rf, own, quarter, 1)
    total = lax.psum(jnp.sum(routed * routed, axis=1), "tp")
    scaled = routed * lax.rsqrt(total / width + EPS)[:, None]
    return (resid_part + scaled * ffn_gain_out).astype(bf16)


def solution(mesh):
    return jax.shard_map(
        per_device,
        mesh=mesh,
        in_specs=(
            P("ep", None),
            P("ep", "tp", None, None),
            P("ep", "tp"),
            P(),
            P(None, "tp"),
            P(None, "tp"),
            P(None, "tp"),
            P(None, "tp"),
            P(None, "tp"),
            P("tp"),
            P("tp"),
            P("tp"),
            P("tp", None),
            P(),
            P(),
            P("ep", None),
            P("ep", None),
            P("ep", None, "tp"),
            P("ep", None, "tp"),
            P("ep", "tp", None),
            P("tp"),
        ),
        out_specs=P("ep", "tp"),
        check_vma=False,
    )
```

profile of v0, /device:TPU:0, one launch (start us, length us, event | category | flops | bytes accessed | tf_op | source)
XLA Modules:
  0.0 91.5 jit_solution(16629815895781907717)
XLA Ops:
  6.5 0.0 copy-start
  6.5 0.0 copy-start.8
  6.6 0.0 copy-start.2
  6.6 0.0 reduce-scatter.2.cloned.1.call-start
  6.6 0.0 copy-start.10
  6.6 1.0 %fusion.22 = f32[16]{0:T(128)S(1)} fusion(bf16[16,1024]{1,0:T(8,128)(2,1)} %param.21), kind=kLoop, calls=%fused_computation.38 | loop fusion | flops 49136 | bytes 32832 | tf_op jit(solution)/shard_map/reduce_sum | solution.py:10
  9.0 0.0 copy-start.4
  9.0 1.2 %convolution_multiply_fusion.2 = f32[16,128]{1,0:T(8,128)S(1)} fusion(bf16[1024,128]{1,0:T(8,128)(2,1)} %param.25, bf16[16,1024]{1,0:T(8,128)(2,1)} %param.21, f32[1024]{0:T(1024)} %param.24, f32[16]{0:T(128)S(1)} %add_rsqrt_fusion.4), kind=kOutput, calls=%fused_computation.14 | convolution fusion | flops 4261888 | bytes 307264 | tf_op jit(solution)/shard_map/dot_general | solution.py:44
  10.2 1.3 %fusion.6 = f32[16]{0:T(128)S(1)} fusion(f32[16,128]{1,0:T(8,128)S(1)} %convolution_multiply_fusion.2, bf16[1024,128]{1,0:T(8,128)(2,1)} %param.26, bf16[16,1024]{1,0:T(8,128)(2,1)} %param.21, f32[1024]{0:T(1024)} %param.24, f32[16]{0:T(128)S(1)} %add_rsqrt_fusion.4), kind=kOutput, calls=%fused_computation.15 | convolution fusion | flops 4263920 | bytes 307328 | tf_op jit(solution)/shard_map/dot_general | solution.py:47
  11.5 0.0 copy-start.7
  11.5 1.0 %fusion.8 = f32[16,1]{0,1:T(1,128)S(1)} fusion(bf16[1024,1]{0,1:T(2,128)(2,1)} %param.28, f32[]{:T(128)} %bitcast.97, bf16[16,1024]{1,0:T(8,128)(2,1)} %param.21, f32[1024]{0:T(1024)} %param.24, f32[16]{0:T(128)S(1)} %add_rsqrt_fusion.4), kind=kOutput, calls=%fused_computation.18 | convolution fusion | flops 98320 | bytes 39044 | tf_op jit(solution)/shard_map/dot_general | solution.py:49
  12.5 0.0 copy-done
  12.5 1.1 %fusion = f32[16,1,256]{2,1,0:T(1,128)S(1)} fusion(f32[16,128,1]{1,2,0:T(1,128)S(1)} %bitcast.101, f32[16,1,128,256]{3,2,1,0:T(8,128)S(1)} %copy-done), kind=kOutput, calls=%fused_computation.1 | convolution fusion | flops 6291456 | bytes 2121728 | tf_op jit(solution)/shard_map/shk,shkv->shv/dot_general | solution.py:57
  13.6 0.0 copy-done.3
  13.6 0.0 copy-done.12
  13.6 0.0 copy-done.13
  13.6 0.0 copy-done.11
  13.6 0.2 fusion.39
  13.9 0.3 multiply_reduce_fusion.3
  14.2 0.2 convolution_convert_fusion.2
  14.5 12.9 %psum.14 = bf16[16,1024]{1,0:T(8,128)(2,1)S(1)} all-reduce(bf16[16,1024]{1,0:T(8,128)(2,1)S(1)} %convolution_convert_fusion.2), channel_id=1, replica_groups=mesh['ep'=8,'tp'=4] {'tp'}, use_global_device_ids=true, to_apply=%region_3.4 | all-reduce | flops 16384 | bytes 65536 | tf_op jit(solution)/shard_map/psum | solution.py:66
  27.4 0.1 fusion.20
  27.5 0.2 multiply_reduce_fusion.1
  27.8 0.1 copy.29
  27.8 0.1 reshape.181
  27.9 0.1 fusion.27
  28.0 0.1 reduce_window_sum.11
  28.2 0.2 select_reduce_fusion
  28.3 0.1 reduce_sum.84
  28.5 0.1 copy.31
  28.5 0.1 fusion.28
  28.6 0.3 convolution_convert_fusion.1
  28.9 0.0 copy-start.9
  28.9 13.8 %all_to_all.10 = bf16[8,16,1024]{2,1,0:T(8,128)(2,1)S(1)} all-to-all(bf16[8,16,1024]{2,1,0:T(8,128)(2,1)S(1)} %bitcast.100), channel_id=1, replica_groups=mesh['ep'=8,'tp'=4] {'ep'}, dimensions={0} | all-to-all | bytes 524288 | tf_op jit(solution)/shard_map/all_to_all | solution.py:90
  42.8 0.0 copy-done.1
  42.8 0.2 convolution_bitcast_fusion.1
  43.0 2.4 %convolution_convert_fusion = bf16[8,16,1024]{2,1,0:T(8,128)(2,1)} fusion(bf16[8,16,1024]{2,1,0:T(8,128)(2,1)S(1)} %all_to_all.10, bf16[1,256,1024]{2,1,0:T(8,128)(2,1)} %param.40, bf16[1,1024,256]{2,1,0:T(8,128)(2,1)} %param.39, f32[8,1,16,256]{3,2,0,1:T(8,128)S(1)} %convolution_bitcast_fusion.1), kind=kOutput, calls=%fused_computation.3 | convolution fusion | flops 134545408 | bytes 1703936 | tf_op jit(solution)/shard_map/secf,efd->secd/dot_general | solution.py:96
  45.4 0.0 reduce-scatter.2.cloned.1.call-update
  45.4 0.1 mul.213
  45.5 19.0 %reduce-scatter.2.cloned.1.call-done = bf16[8,16,256]{2,1,0:T(8,128)(2,1)} async-done(((bf16[8,16,1024]{2,1,0:T(8,128)(2,1)}), bf16[8,16,256]{2,1,0:T(8,128)(2,1)}) %reduce-scatter.2.cloned.1.call-update) | async-done | bytes 65552 | tf_op jit(solution)/shard_map/reduce_scatter | solution.py:99
  64.5 5.5 %all-to-all-start.1 = ((bf16[8,16,256]{2,1,0:T(8,128)(2,1)}), bf16[8,16,256]{2,1,0:T(8,128)(2,1)S(1)}, u32[]{:S(2)}, u32[]{:S(2)}) async-start(bf16[8,16,256]{2,1,0:T(8,128)(2,1)} %reduce-scatter.2.cloned.1.call-done), calls=%async_computation.2 | async-start | bytes 131072 | tf_op jit(solution)/shard_map/all_to_all | solution.py:103
  70.1 0.1 copy.28
  70.2 6.8 %all-to-all-done.1 = bf16[8,16,256]{2,1,0:T(8,128)(2,1)S(1)} async-done(((bf16[8,16,256]{2,1,0:T(8,128)(2,1)}), bf16[8,16,256]{2,1,0:T(8,128)(2,1)S(1)}, u32[]{:S(2)}, u32[]{:S(2)}) %all-to-all-start.1) | async-done | bytes 65568 | tf_op jit(solution)/shard_map/all_to_all | solution.py:103
  77.0 0.8 gather_fusion
  77.8 0.1 multiply_reduce_fusion
  77.9 0.1 multiply_reduce_fusion.2
  78.0 5.9 %psum.15 = f32[16]{0:T(128)S(1)} all-reduce(f32[16]{0:T(128)S(1)} %multiply_reduce_fusion.2), channel_id=1, replica_groups=mesh['ep'=8,'tp'=4] {'tp'}, use_global_device_ids=true, to_apply=%region_12.13 | all-reduce | flops 16 | bytes 128 | tf_op jit(solution)/shard_map/psum | solution.py:110
  84.0 0.7 add_convert_fusion
  (25 shorter events, 0.1 us)
Async XLA Ops:
  6.5 6.0 %copy-start = (f32[16,1,128,256]{3,2,1,0:T(8,128)S(1)}, f32[16,1,128,256]{3,2,1,0:T(8,128)}, u32[]{:S(2)}) copy-start(f32[16,1,128,256]{3,2,1,0:T(8,128)} %param.22) | copy-start | bytes 6291460
  6.5 7.1 %copy-start.3 = (bf16[16,1024]{1,0:T(8,128)(2,1)S(1)}, bf16[16,1024]{1,0:T(8,128)(2,1)}, u32[]{:S(2)}) copy-start(bf16[16,1024]{1,0:T(8,128)(2,1)} %param.21) | copy-start | bytes 98308
  6.5 7.1 %copy-start.12 = (f32[1024]{0:T(1024)S(1)}, f32[1024]{0:T(1024)}, u32[]{:S(2)}) copy-start(f32[1024]{0:T(1024)} %param.24) | copy-start | bytes 12292
  6.5 7.1 %copy-start.13 = (f32[16,1]{0,1:T(1,128)S(1)}, f32[16,1]{0,1:T(1,128)}, u32[]{:S(2)}) copy-start(f32[16,1]{0,1:T(1,128)} %param.23) | copy-start | bytes 196
  6.5 7.1 %copy-start.11 = (bf16[1024,1]{0,1:T(2,128)(2,1)S(1)}, bf16[1024,1]{0,1:T(2,128)(2,1)}, u32[]{:S(2)}) copy-start(bf16[1024,1]{0,1:T(2,128)(2,1)} %param.29) | copy-start | bytes 6148
  6.5 7.7 %copy-start.8 = (f32[256]{0:T(256)S(1)}, f32[256]{0:T(256)}, u32[]{:S(2)}) copy-start(f32[256]{0:T(256)} %param.32) | copy-start | bytes 3076
  6.6 7.7 %copy-start.2 = (bf16[256,1024]{1,0:T(8,128)(2,1)S(1)}, bf16[256,1024]{1,0:T(8,128)(2,1)}, u32[]{:S(2)}) copy-start(bf16[256,1024]{1,0:T(8,128)(2,1)} %param.33) | copy-start | bytes 1572868
  6.6 58.0 %reduce-scatter.2.cloned.1.call-start = ((), (), s32[]{:S(2)}) async-start(), calls=%async_computation.3 | async-start | bytes 327680 | tf_op jit(solution)/shard_map/reduce_scatter | solution.py:99
  6.6 7.3 %copy-start.10 = (bf16[1024,256]{1,0:T(8,128)(2,1)S(1)}, bf16[1024,256]{1,0:T(8,128)(2,1)}, u32[]{:S(2)}) copy-start(bf16[1024,256]{1,0:T(8,128)(2,1)} %param.27) | copy-start | bytes 1572868
  9.0 18.5 %copy-start.4 = (f32[1024]{0:T(1024)S(1)}, f32[1024]{0:T(1024)}, u32[]{:S(2)}) copy-start(f32[1024]{0:T(1024)} %param.34) | copy-start | bytes 12292
  10.2 17.6 %copy-start.5 = (s32[16,6]{0,1:T(8,128)S(1)}, s32[16,6]{0,1:T(8,128)}, u32[]{:S(2)}) copy-start(s32[16,6]{0,1:T(8,128)} %param.36) | copy-start | bytes 1156
  11.5 17.1 %copy-start.7 = (f32[1024]{0:T(1024)S(1)}, f32[1024]{0:T(1024)}, u32[]{:S(2)}) copy-start(f32[1024]{0:T(1024)} %param.35) | copy-start | bytes 12292
  12.5 30.2 %copy-start.1 = (bf16[1,1024,256]{2,1,0:T(8,128)(2,1)S(1)}, bf16[1,1024,256]{2,1,0:T(8,128)(2,1)}, u32[]{:S(2)}) copy-start(bf16[1,1024,256]{2,1,0:T(8,128)(2,1)} %param.38) | copy-start | bytes 1572868
  27.7 42.3 %copy-start.6 = (f32[16,6]{0,1:T(8,128)S(1)}, f32[16,6]{0,1:T(8,128)}, u32[]{:S(2)}) copy-start(f32[16,6]{0,1:T(8,128)} %param.37) | copy-start | bytes 1156
  28.9 55.0 %copy-start.9 = (f32[256]{0:T(256)S(1)}, f32[256]{0:T(256)}, u32[]{:S(2)}) copy-start(f32[256]{0:T(256)} %param.41) | copy-start | bytes 3076
  64.5 12.4 %all-to-all-start.1 = ((bf16[8,16,256]{2,1,0:T(8,128)(2,1)}), bf16[8,16,256]{2,1,0:T(8,128)(2,1)S(1)}, u32[]{:S(2)}, u32[]{:S(2)}) async-start(bf16[8,16,256]{2,1,0:T(8,128)(2,1)} %reduce-scatter.2.cloned.1.call-done), calls=%async_computation.2 | async-start | bytes 131072 | tf_op jit(solution)/shard_map/all_to_all | solution.py:103
Sparse Core Ops, SparseCore 0:
  45.5 18.9 reduce-scatter.1
where the time goes:
time: 91.9 us; the launch traced here: 91.5 us
  blocking collectives  32.7 us (36%)
  waiting for transfers between devices  25.8 us (28%)
  between operations  15 us (16%)
  matrix products  8.26 us (9%)
  starting transfers between devices  5.57 us (6%)
  other arithmetic  2.83 us (3%)
  local copies, waits for them, and re-layouts  1.35 us (1%)
    reduce_scatter x1, waiting for transfers between devices, per_device(): lax.psum_scatter(part.astype(jnp.bfloat16), 'tp', scatter_dimension=2, ti...  19 us
    all_to_all x1, blocking collectives, per_device(): lax.all_to_all(outbound, 'ep', split_axis=0, concat_axis=0, tiled=True)  13.8 us
    psum x1, blocking collectives, per_device(): lax.psum(partial_value.astype(jnp.bfloat16), 'tp').astype(jnp.float32)  12.9 us
    all_to_all x1, waiting for transfers between devices, per_device(): lax.all_to_all(done, 'ep', split_axis=0, concat_axis=0, tiled=True)  6.79 us
    psum x1, blocking collectives, per_device(): total = lax.psum(jnp.sum(routed * routed, axis=1), 'tp')  5.95 us
    all_to_all x1, starting transfers between devices, per_device(): lax.all_to_all(done, 'ep', split_axis=0, concat_axis=0, tiled=True)  5.53 us
    dot_general x1, matrix products, per_device(): jnp.einsum('secf,efd->secd', act, expert_down, preferred_element_type=f32)  2.4 us
  transfers between devices with their start and end apart: 2, of which 2 were waited for; matrix products, arithmetic and copies ran while one was open for 0% of the time, Pallas kernels for 0%

commit v1 on v0

--- a/solution.py
+++ b/solution.py
@@ -63,7 +63,9 @@
         .reshape(seqs, heads * value_dim)
     )
     partial_value = jnp.dot(headout, w_output, preferred_element_type=f32)
-    mixed = lax.psum(partial_value.astype(jnp.bfloat16), "tp").astype(jnp.float32)
+    mixed = jnp.sum(lax.all_gather(partial_value.astype(jnp.bfloat16), "tp"), axis=0).astype(
+        jnp.float32
+    )
     resid = (xf + mixed * rms_scale(mixed) * mix_gain_out).astype(bf16)
     rf = resid.astype(f32)
     ffn_in = (rf * rms_scale(rf) * ffn_gain_in).astype(bf16)

time: 91.9 us -> 87.2 us (0.949)
  blocking collectives: 32.7 us -> 27.9 us
    psum x1 -> x0, blocking collectives: 12.9 us -> none  [per_device(): lax.psum(partial_value.astype(jnp.bfloat16), 'tp').astype(jnp.float32)]
    all_gather x0 -> x1, blocking collectives: none -> 6.53 us  [per_device(): lax.all_gather(partial_value.astype(jnp.bfloat16), 'tp')]
    all_to_all x1, blocking collectives: 13.8 us -> 15.4 us  [per_device(): lax.all_to_all(outbound, 'ep', split_axis=0, concat_axis=0, tiled=True)]
where the time goes in v1:
time: 87.2 us; the launch traced here: 86.8 us
  blocking collectives  27.9 us (32%)
  waiting for transfers between devices  26 us (30%)
  between operations  15 us (17%)
  matrix products  8.26 us (9%)
  starting transfers between devices  5.53 us (6%)
  other arithmetic  2.85 us (3%)
  local copies, waits for them, and re-layouts  1.35 us (2%)
    reduce_scatter x1, waiting for transfers between devices, per_device(): lax.psum_scatter(part.astype(jnp.bfloat16), 'tp', scatter_dimension=2, ti...  19.1 us
    all_to_all x1, blocking collectives, per_device(): lax.all_to_all(outbound, 'ep', split_axis=0, concat_axis=0, tiled=True)  15.4 us
    all_to_all x1, waiting for transfers between devices, per_device(): lax.all_to_all(done, 'ep', split_axis=0, concat_axis=0, tiled=True)  6.79 us
    all_gather x1, blocking collectives, per_device(): lax.all_gather(partial_value.astype(jnp.bfloat16), 'tp')  6.53 us
    psum x1, blocking collectives, per_device(): total = lax.psum(jnp.sum(routed * routed, axis=1), 'tp')  5.97 us
    all_to_all x1, starting transfers between devices, per_device(): lax.all_to_all(done, 'ep', split_axis=0, concat_axis=0, tiled=True)  5.49 us
    dot_general x1, matrix products, per_device(): jnp.einsum('secf,efd->secd', act, expert_down, preferred_element_type=f32)  2.4 us
  transfers between devices with their start and end apart: 2, of which 2 were waited for; matrix products, arithmetic and copies ran while one was open for 0% of the time, Pallas kernels for 0%

profile of v1, /device:TPU:0, one launch (start us, length us, event | category | flops | bytes accessed | tf_op | source)
XLA Modules:
  0.0 86.8 jit_solution(4864303460217692782)
XLA Ops:
  6.5 0.0 copy-start
  6.5 0.0 copy-start.8
  6.6 0.0 copy-start.2
  6.6 0.0 reduce-scatter.2.cloned.1.call-start
  6.6 0.0 copy-start.10
  6.6 1.0 %fusion.22 = f32[16]{0:T(128)S(1)} fusion(bf16[16,1024]{1,0:T(8,128)(2,1)} %param.21), kind=kLoop, calls=%fused_computation.38 | loop fusion | flops 49136 | bytes 32832 | tf_op jit(solution)/shard_map/reduce_sum | solution.py:10
  9.0 1.2 %convolution_multiply_fusion.2 = f32[16,128]{1,0:T(8,128)S(1)} fusion(bf16[1024,128]{1,0:T(8,128)(2,1)} %param.25, bf16[16,1024]{1,0:T(8,128)(2,1)} %param.21, f32[1024]{0:T(1024)} %param.24, f32[16]{0:T(128)S(1)} %add_rsqrt_fusion.4), kind=kOutput, calls=%fused_computation.14 | convolution fusion | flops 4261888 | bytes 307264 | tf_op jit(solution)/shard_map/dot_general | solution.py:44
  10.2 1.3 %fusion.6 = f32[16]{0:T(128)S(1)} fusion(f32[16,128]{1,0:T(8,128)S(1)} %convolution_multiply_fusion.2, bf16[1024,128]{1,0:T(8,128)(2,1)} %param.26, bf16[16,1024]{1,0:T(8,128)(2,1)} %param.21, f32[1024]{0:T(1024)} %param.24, f32[16]{0:T(128)S(1)} %add_rsqrt_fusion.4), kind=kOutput, calls=%fused_computation.15 | convolution fusion | flops 4263920 | bytes 307328 | tf_op jit(solution)/shard_map/dot_general | solution.py:47
  11.5 0.0 copy-start.5
  11.5 1.0 %fusion.8 = f32[16,1]{0,1:T(1,128)S(1)} fusion(bf16[1024,1]{0,1:T(2,128)(2,1)} %param.28, f32[]{:T(128)} %bitcast.98, bf16[16,1024]{1,0:T(8,128)(2,1)} %param.21, f32[1024]{0:T(1024)} %param.24, f32[16]{0:T(128)S(1)} %add_rsqrt_fusion.4), kind=kOutput, calls=%fused_computation.18 | convolution fusion | flops 98320 | bytes 39044 | tf_op jit(solution)/shard_map/dot_general | solution.py:49
  12.5 0.0 copy-done
  12.5 1.1 %fusion = f32[16,1,256]{2,1,0:T(1,128)S(1)} fusion(f32[16,128,1]{1,2,0:T(1,128)S(1)} %bitcast.103, f32[16,1,128,256]{3,2,1,0:T(8,128)S(1)} %copy-done), kind=kOutput, calls=%fused_computation.1 | convolution fusion | flops 6291456 | bytes 2121728 | tf_op jit(solution)/shard_map/shk,shkv->shv/dot_general | solution.py:57
  13.6 0.0 copy-done.3
  13.6 0.0 copy-done.12
  13.6 0.0 copy-done.13
  13.6 0.2 fusion.39
  13.9 0.3 multiply_reduce_fusion.3
  14.2 0.0 copy-done.8
  14.2 0.0 copy-done.2
  14.2 0.2 convolution_convert_fusion.2
  14.5 6.5 %all-gather = bf16[64,1024]{1,0:T(8,128)(2,1)S(1)} all-gather(bf16[16,1024]{1,0:T(8,128)(2,1)S(1)} %convolution_convert_fusion.2), channel_id=2, replica_groups=mesh['ep'=8,'tp'=4] {'tp'}, dimensions={0}, use_global_device_ids=true | all-gather | bytes 163840 | tf_op jit(solution)/shard_map/all_gather | solution.py:66
  21.0 0.1 fusion.20
  21.1 0.2 multiply_reduce_fusion.1
  21.4 0.1 copy.29
  21.5 0.1 reshape.181
  21.5 0.1 fusion.27
  21.6 0.1 reduce_window_sum.11
  21.8 0.2 select_reduce_fusion
  22.0 0.1 reduce_sum.97
  22.1 0.1 copy.31
  22.1 0.1 fusion.28
  22.2 0.0 copy-done.7
  22.3 0.3 convolution_convert_fusion.1
  22.5 0.0 copy-start.9
  22.5 15.4 %all_to_all.10 = bf16[8,16,1024]{2,1,0:T(8,128)(2,1)S(1)} all-to-all(bf16[8,16,1024]{2,1,0:T(8,128)(2,1)S(1)} %bitcast.101), channel_id=1, replica_groups=mesh['ep'=8,'tp'=4] {'ep'}, dimensions={0} | all-to-all | bytes 524288 | tf_op jit(solution)/shard_map/all_to_all | solution.py:92
  37.9 0.2 convolution_bitcast_fusion.1
  38.2 2.4 %convolution_convert_fusion = bf16[8,16,1024]{2,1,0:T(8,128)(2,1)} fusion(bf16[8,16,1024]{2,1,0:T(8,128)(2,1)S(1)} %all_to_all.10, bf16[1,256,1024]{2,1,0:T(8,128)(2,1)} %param.40, bf16[1,1024,256]{2,1,0:T(8,128)(2,1)} %param.39, f32[8,1,16,256]{3,2,0,1:T(8,128)S(1)} %convolution_bitcast_fusion.1), kind=kOutput, calls=%fused_computation.3 | convolution fusion | flops 134545408 | bytes 1703936 | tf_op jit(solution)/shard_map/secf,efd->secd/dot_general | solution.py:98
  40.6 0.0 reduce-scatter.2.cloned.1.call-update
  40.6 0.1 mul.213
  40.7 19.1 %reduce-scatter.2.cloned.1.call-done = bf16[8,16,256]{2,1,0:T(8,128)(2,1)} async-done(((bf16[8,16,1024]{2,1,0:T(8,128)(2,1)}), bf16[8,16,256]{2,1,0:T(8,128)(2,1)}) %reduce-scatter.2.cloned.1.call-update) | async-done | bytes 65552 | tf_op jit(solution)/shard_map/reduce_scatter | solution.py:101
  59.8 5.5 %all-to-all-start.1 = ((bf16[8,16,256]{2,1,0:T(8,128)(2,1)}), bf16[8,16,256]{2,1,0:T(8,128)(2,1)S(1)}, u32[]{:S(2)}, u32[]{:S(2)}) async-start(bf16[8,16,256]{2,1,0:T(8,128)(2,1)} %reduce-scatter.2.cloned.1.call-done), calls=%async_computation.2 | async-start | bytes 131072 | tf_op jit(solution)/shard_map/all_to_all | solution.py:105
  65.3 0.1 copy.28
  65.4 6.8 %all-to-all-done.1 = bf16[8,16,256]{2,1,0:T(8,128)(2,1)S(1)} async-done(((bf16[8,16,256]{2,1,0:T(8,128)(2,1)}), bf16[8,16,256]{2,1,0:T(8,128)(2,1)S(1)}, u32[]{:S(2)}, u32[]{:S(2)}) %all-to-all-start.1) | async-done | bytes 65568 | tf_op jit(solution)/shard_map/all_to_all | solution.py:105
  72.2 0.8 gather_fusion
  73.0 0.1 multiply_reduce_fusion
  73.2 0.1 multiply_reduce_fusion.2
  73.3 6.0 %psum.7 = f32[16]{0:T(128)S(1)} all-reduce(f32[16]{0:T(128)S(1)} %multiply_reduce_fusion.2), channel_id=1, replica_groups=mesh['ep'=8,'tp'=4] {'tp'}, use_global_device_ids=true, to_apply=%region_12.13 | all-reduce | flops 16 | bytes 128 | tf_op jit(solution)/shard_map/psum | solution.py:112
  79.3 0.7 add_convert_fusion
  (26 shorter events, 0.1 us)
Async XLA Ops:
  6.5 6.0 %copy-start = (f32[16,1,128,256]{3,2,1,0:T(8,128)S(1)}, f32[16,1,128,256]{3,2,1,0:T(8,128)}, u32[]{:S(2)}) copy-start(f32[16,1,128,256]{3,2,1,0:T(8,128)} %param.22) | copy-start | bytes 6291460
  6.5 7.1 %copy-start.3 = (bf16[16,1024]{1,0:T(8,128)(2,1)S(1)}, bf16[16,1024]{1,0:T(8,128)(2,1)}, u32[]{:S(2)}) copy-start(bf16[16,1024]{1,0:T(8,128)(2,1)} %param.21) | copy-start | bytes 98308
  6.5 7.1 %copy-start.12 = (f32[1024]{0:T(1024)S(1)}, f32[1024]{0:T(1024)}, u32[]{:S(2)}) copy-start(f32[1024]{0:T(1024)} %param.24) | copy-start | bytes 12292
  6.5 7.1 %copy-start.13 = (f32[16,1]{0,1:T(1,128)S(1)}, f32[16,1]{0,1:T(1,128)}, u32[]{:S(2)}) copy-start(f32[16,1]{0,1:T(1,128)} %param.23) | copy-start | bytes 196
  6.5 7.1 %copy-start.11 = (bf16[1024,1]{0,1:T(2,128)(2,1)S(1)}, bf16[1024,1]{0,1:T(2,128)(2,1)}, u32[]{:S(2)}) copy-start(bf16[1024,1]{0,1:T(2,128)(2,1)} %param.29) | copy-start | bytes 6148
  6.5 7.7 %copy-start.8 = (f32[256]{0:T(256)S(1)}, f32[256]{0:T(256)}, u32[]{:S(2)}) copy-start(f32[256]{0:T(256)} %param.32) | copy-start | bytes 3076
  6.6 7.7 %copy-start.2 = (bf16[256,1024]{1,0:T(8,128)(2,1)S(1)}, bf16[256,1024]{1,0:T(8,128)(2,1)}, u32[]{:S(2)}) copy-start(bf16[256,1024]{1,0:T(8,128)(2,1)} %param.33) | copy-start | bytes 1572868
  6.6 53.3 %reduce-scatter.2.cloned.1.call-start = ((), (), s32[]{:S(2)}) async-start(), calls=%async_computation.3 | async-start | bytes 327680 | tf_op jit(solution)/shard_map/reduce_scatter | solution.py:101
  6.6 7.2 %copy-start.10 = (bf16[1024,256]{1,0:T(8,128)(2,1)S(1)}, bf16[1024,256]{1,0:T(8,128)(2,1)}, u32[]{:S(2)}) copy-start(bf16[1024,256]{1,0:T(8,128)(2,1)} %param.27) | copy-start | bytes 1572868
  10.2 11.0 %copy-start.4 = (f32[1024]{0:T(1024)S(1)}, f32[1024]{0:T(1024)}, u32[]{:S(2)}) copy-start(f32[1024]{0:T(1024)} %param.34) | copy-start | bytes 12292
  11.5 9.9 %copy-start.5 = (s32[16,6]{0,1:T(8,128)S(1)}, s32[16,6]{0,1:T(8,128)}, u32[]{:S(2)}) copy-start(s32[16,6]{0,1:T(8,128)} %param.36) | copy-start | bytes 1156
  12.5 9.8 %copy-start.7 = (f32[1024]{0:T(1024)S(1)}, f32[1024]{0:T(1024)}, u32[]{:S(2)}) copy-start(f32[1024]{0:T(1024)} %param.35) | copy-start | bytes 12292
  12.5 25.4 %copy-start.1 = (bf16[1,1024,256]{2,1,0:T(8,128)(2,1)S(1)}, bf16[1,1024,256]{2,1,0:T(8,128)(2,1)}, u32[]{:S(2)}) copy-start(bf16[1,1024,256]{2,1,0:T(8,128)(2,1)} %param.38) | copy-start | bytes 1572868
  21.3 44.0 %copy-start.6 = (f32[16,6]{0,1:T(8,128)S(1)}, f32[16,6]{0,1:T(8,128)}, u32[]{:S(2)}) copy-start(f32[16,6]{0,1:T(8,128)} %param.37) | copy-start | bytes 1156
  22.5 56.7 %copy-start.9 = (f32[256]{0:T(256)S(1)}, f32[256]{0:T(256)}, u32[]{:S(2)}) copy-start(f32[256]{0:T(256)} %param.41) | copy-start | bytes 3076
  59.8 12.4 %all-to-all-start.1 = ((bf16[8,16,256]{2,1,0:T(8,128)(2,1)}), bf16[8,16,256]{2,1,0:T(8,128)(2,1)S(1)}, u32[]{:S(2)}, u32[]{:S(2)}) async-start(bf16[8,16,256]{2,1,0:T(8,128)(2,1)} %reduce-scatter.2.cloned.1.call-done), calls=%async_computation.2 | async-start | bytes 131072 | tf_op jit(solution)/shard_map/all_to_all | solution.py:105
Sparse Core Ops, SparseCore 0:
  40.7 19.0 reduce-scatter.1
